TPU v7x, 512 devices: a whole 4x8x8 slice. The times are simulated.
512 devices in a mesh: sp: 64 (over z, y), tp: 8 (over x, core).
Axes of the slice: x: 4, y: 8, z: 8, core: 2. Of those that a mesh axis runs over, the one named last changes fastest.
Arguments:
- block_input: bfloat16 [32768, 2048], P('sp'), may hold values from -6 to 6
- value_weight: bfloat16 [2048, 2048], P(None, 'tp'), may hold values from -0.125 to 0.125
- queries: bfloat16 [32768, 1024], P('sp', 'tp'), may hold values from -0.5 to 0.5
- key_rows: bfloat16 [32768, 1024], P('sp', 'tp'), may hold values from -0.5 to 0.5
- log_decay: float32 [32768, 32], P('sp', 'tp'), may hold values from -0.125 to 0, as said below
- out_grad: bfloat16 [32768, 2048], P('sp', 'tp'), may hold values from -6 to 6
Outputs:
- query_grad: float32 [32768, 1024], P('sp', 'tp')
- key_grad: float32 [32768, 1024], P('sp', 'tp')
- decay_grad: float32 [32768, 32], P('sp', 'tp')
- weight_grad: float32 [2048, 2048], P('sp', 'tp')
- row_norms: float32 [2048], P('sp')
Inputs may be any that keep to these rules, and one draw needn't show every extreme that they name: `log_decay`: log decays of each position and head, never positive.
All inputs are finite; a program needn't handle non-finite values.
Results may differ from a plain program's by a relative error of at most 0.013.
Values sent between devices are 32-bit elements; how exact they have to be, the bound alone decides.
A program may use at most 64 MiB of HBM per device.

v0:
```python
import jax
import jax.numpy as jnp
from jax import lax
from jax.sharding import Mesh
from jax.sharding import PartitionSpec as P

HEAD_DIM = 64
STATE = 128
SPAN = 128
SP = ("sp_0", "sp_1")


exact_mode = lax.Precision.HIGHEST


def filled_with(array, identity):
    return jax.tree.map(
        lambda part, zero: jnp.zeros_like(part) + jnp.asarray(zero, part.dtype), array, identity
    )


def prefix_by_axis(array, axes, combine, identity, reverse):
    before = start = filled_with(array, identity)
    subtotal = array
    for axis in reversed(axes):
        size, position = (lax.axis_size(axis), lax.axis_index(axis))
        pieces = jax.tree.map(lambda part: lax.all_gather(part, axis), subtotal)
        inside, subtotal = (start, start)
        for k in reversed(range(size)) if reverse else range(size):
            passed = k > position if reverse else k < position
            subtotal = combine(subtotal, jax.tree.map(lambda part: part[k], pieces))
            inside = jax.tree.map(lambda new, old: jnp.where(passed, new, old), subtotal, inside)
        before = combine(inside, before)
    return before


def in_blocks(array, dim, size):
    lengths = array.shape
    blocks = array.reshape(*lengths[:dim], size, lengths[dim] // size, *lengths[dim + 1 :])
    return jnp.moveaxis(blocks, dim, 0)


def summed_on_arrival(array, axis, dim):
    size = lax.axis_size(axis)
    blocks = lax.all_to_all(in_blocks(array, dim, size), axis, 0, 0, tiled=True)
    return jnp.sum(blocks, axis=0)


def block_step(memory, pieces):
    queries, key_rows, decays, values = pieces
    length = decays.shape[0]
    cumulative = jnp.cumsum(decays, axis=0)
    causal = (lax.iota(jnp.int32, length)[:, None] >= lax.iota(jnp.int32, length)[None, :])[
        :, :, None, None
    ]
    log_gap = cumulative[:, None] - cumulative[None, :]
    weights = jnp.where(causal, jnp.exp(jnp.where(causal, log_gap, 0.0)), 0.0)
    scores = jnp.einsum("sgn,rgn->srg", queries, key_rows, precision=exact_mode)
    within = jnp.einsum(
        "srgj,rgjp->sgjp", scores[..., None] * weights, values, precision=exact_mode
    )
    carried = (
        jnp.einsum("sgn,gjpn->sgjp", queries, memory, precision=exact_mode)
        * jnp.exp(cumulative)[..., None]
    )
    to_end = jnp.exp(cumulative[-1] - cumulative)
    fresh_state = jnp.einsum(
        "rgn,rgjp->gjpn", key_rows, values * to_end[..., None], precision=exact_mode
    )
    new_memory = jnp.exp(cumulative[-1])[..., None, None] * memory + fresh_state
    return (new_memory, within + carried)


def combine(earlier, later):
    early_log, early_state = earlier
    late_log, late_state = later
    return (early_log + late_log, jnp.exp(late_log)[..., None, None] * early_state + late_state)


def on_device(block_input, value_weight, queries, key_rows, log_decay, out_grad):
    rows = block_input.shape[0]
    heads = log_decay.shape[1]
    groups = queries.shape[1] // STATE
    per_group = heads // groups
    blocks = rows // SPAN
    values = jnp.dot(block_input, value_weight, preferred_element_type=jnp.float32).astype(
        jnp.bfloat16
    )
    query_f = queries.astype(jnp.float32).reshape(rows, groups, STATE)
    key_f = key_rows.astype(jnp.float32).reshape(rows, groups, STATE)
    decays = log_decay.reshape(rows, groups, per_group)
    value_f = values.astype(jnp.float32).reshape(rows, groups, per_group, HEAD_DIM)
    grad_f = out_grad.astype(jnp.float32).reshape(rows, groups, per_group, HEAD_DIM)
    cumulative = jnp.cumsum(decays, axis=0)
    shard_log = cumulative[-1]
    own_state = jnp.einsum(
        "tgn,tgjp->gjpn",
        key_f,
        value_f * jnp.exp(shard_log - cumulative)[..., None],
        precision=exact_mode,
    )
    own_grad = jnp.einsum(
        "tgn,tgjp->gjpn", query_f, grad_f * jnp.exp(cumulative)[..., None], precision=exact_mode
    )
    identity = (jnp.zeros_like(shard_log), jnp.zeros_like(own_state))
    before_log, state_in = prefix_by_axis((shard_log, own_state), SP, combine, identity, False)
    unused, state_grad = prefix_by_axis((shard_log, own_grad), SP, combine, identity, True)

    def local_pass(query_in, key_in, decay_in, value_in):
        pieces = (
            query_in.reshape(blocks, SPAN, groups, STATE),
            key_in.reshape(blocks, SPAN, groups, STATE),
            decay_in.reshape(blocks, SPAN, groups, per_group),
            value_in.reshape(blocks, SPAN, groups, per_group, HEAD_DIM),
        )
        final, outputs = lax.scan(block_step, state_in, pieces)
        return (outputs, final)

    results, pullback = jax.vjp(local_pass, query_f, key_f, decays, value_f)
    query_grad, key_grad, decay_grad, value_grad = pullback(
        (grad_f.reshape(blocks, SPAN, groups, per_group, HEAD_DIM), state_grad)
    )
    rounded_grad = value_grad.reshape(rows, heads * HEAD_DIM).astype(jnp.bfloat16)
    weight_grad = summed_on_arrival(
        lax.dot_general(
            block_input, rounded_grad, (((0,), (0,)), ((), ())), preferred_element_type=jnp.float32
        ),
        SP,
        0,
    )
    row_norms = lax.psum(jnp.sum(weight_grad * weight_grad, axis=1), "tp")
    return (
        query_grad.reshape(rows, groups * STATE),
        key_grad.reshape(rows, groups * STATE),
        decay_grad.reshape(rows, heads),
        weight_grad,
        row_norms,
    )


def solution(mesh):
    split = Mesh(mesh.devices.reshape(8, 8, mesh.shape["tp"]), ("sp_0", "sp_1", "tp"))
    return jax.shard_map(
        on_device,
        mesh=split,
        in_specs=(P(SP, None), P(None, "tp"), P(SP, "tp"), P(SP, "tp"), P(SP, "tp"), P(SP, "tp")),
        out_specs=(P(SP, "tp"), P(SP, "tp"), P(SP, "tp"), P(SP, "tp"), P(SP)),
        check_vma=False,
    )
```

profile of v0, /device:TPU:1, one launch (start us, length us, event | category | flops | bytes accessed | tf_op | source)
XLA Modules:
  0.0 365.3 jit_solution(13655656036096398556)
XLA Ops:
  10.8 2.0 bitcast_multiply_fusion.5
  16.4 13.8 %all_gather.32 = f32[8,1,4]{2,1,0:T(1,128)S(1)} all-gather(f32[1,1,4]{2,1,0:T(1,128)S(1)} %get-tuple-element.1260), channel_id=1, replica_groups=mesh['sp_0'=8,'sp_1'=8,'tp'=8] {'sp_1'}, dimensions={0}, use_global_device_ids=true | all-gather | bytes 144 | tf_op jit(solution)/shard_map/all_gather | solution.py:27
  30.7 24.7 %all-gather.13.cloned.1.call-done = f32[32,64,128]{2,1,0:T(8,128)} async-done(((f32[4,64,128]{2,1,0:T(8,128)}), f32[32,64,128]{2,1,0:T(8,128)}) %all-gather.13.cloned.1.call-update) | async-done | bytes 1048592 | tf_op jit(solution)/shard_map/all_gather | solution.py:27
  55.5 2.1 bitcast_add_fusion.8
  63.9 13.5 %all_gather.37 = f32[8,1,4]{2,1,0:T(1,128)S(1)} all-gather(f32[1,1,4]{2,1,0:T(1,128)S(1)} %get-tuple-element.1273), channel_id=1, replica_groups=mesh['sp_0'=8,'sp_1'=8,'tp'=8] {'sp_0'}, dimensions={0}, use_global_device_ids=true | all-gather | bytes 144 | tf_op jit(solution)/shard_map/all_gather | solution.py:27
  77.4 11.1 %all_gather.33 = f32[8,1,4]{2,1,0:T(1,128)S(1)} all-gather(f32[1,1,4]{2,1,0:T(1,128)S(1)} %get-tuple-element.1274), channel_id=1, replica_groups=mesh['sp_0'=8,'sp_1'=8,'tp'=8] {'sp_0'}, dimensions={0}, use_global_device_ids=true | all-gather | bytes 144 | tf_op jit(solution)/shard_map/all_gather | solution.py:27
  89.3 8.0 %all-gather.11.cloned.1.call-done = f32[32,64,128]{2,1,0:T(8,128)} async-done(((f32[4,64,128]{2,1,0:T(8,128)}), f32[32,64,128]{2,1,0:T(8,128)}) %all-gather.11.cloned.1.call-update) | async-done | bytes 1048592 | tf_op jit(solution)/shard_map/all_gather | solution.py:27
  97.3 2.1 bitcast_add_fusion.24
  99.4 41.1 %all-gather.9.cloned.1.call-done = f32[8,1,4,64,128]{4,3,2,1,0:T(8,128)} async-done(((f32[1,1,4,64,128]{4,3,2,1,0:T(8,128)}), f32[8,1,4,64,128]{4,3,2,1,0:T(8,128)}) %all-gather.9.cloned.1.call-update) | async-done | bytes 1048592 | tf_op jit(solution)/shard_map/all_gather | solution.py:27
  140.5 2.0 fusion.94
  142.5 42.4 %while.67 = (s32[]{:T(128)}, f32[1,4,64,128]{3,2,1,0:T(8,128)S(1)}, f32[4,128,128,1,4]{2,4,3,1,0:T(4,128)}, f32[4,128,128,1,4]{2,4,3,1,0:T(4,128)}, f32[4,128,12...) while((s32[]{:T(128)}, f32[1,4,64,128]{3,2,1,0:T(8,128)S(1)}, ...), condition=%wide.region_4.5_spmd.clone.clone.clone, body=%wide.region_2.4_spmd.clone.clone.sunk.clone | while | flops 126288896 | bytes 2828605 | solution.py:116
  143.7 1.7 bitcast_dynamic-update-slice_fusion.6
  154.3 1.8 bitcast_dynamic-update-slice_fusion.6
  164.8 1.7 bitcast_dynamic-update-slice_fusion.6
  175.4 1.7 bitcast_dynamic-update-slice_fusion.6
  186.3 2.0 fusion.105
  189.7 84.8 %while.68 = (s32[]{:T(128)}, f32[1,4,64,128]{3,2,1,0:T(8,128)S(1)}, f32[4,128,1,128]{3,1,2,0:T(8,128)}, f32[4,128,1,128]{3,1,2,0:T(8,128)}, f32[4,128,1,4]{3,2,1...) while((s32[]{:T(128)}, f32[1,4,64,128]{3,2,1,0:T(8,128)S(1)}, ...), condition=%wide.region_14.15_spmd.clone.clone.clone, body=%wide.region_5.14_spmd.clone.clone.sunk.clone | while | flops 353324032 | bytes 8525933 | solution.py:116
  193.9 2.2 fusion.263
  207.7 1.9 fusion.265
  215.1 2.2 fusion.263
  226.9 1.7 fusion.264
  228.8 1.9 fusion.265
  236.3 2.2 fusion.263
  250.1 1.9 fusion.265
  257.5 2.2 fusion.263
  271.2 1.9 fusion.265
  275.7 2.0 convolution_bitcast_fusion.9
  277.7 2.9 copy.116
  280.6 10.6 %all-to-all-start = ((f32[64,32,256]{2,1,0:T(8,128)}), f32[64,32,256]{2,1,0:T(8,128)}, u32[]{:S(2)}, u32[]{:S(2)}) async-start(f32[64,32,256]{2,1,0:T(8,128)} %bitcast.853), calls=%async_computation | async-start | bytes 4194304 | tf_op jit(solution)/shard_map/all_to_all | solution.py:45
  292.0 43.9 %all-to-all-done = f32[64,32,256]{2,1,0:T(8,128)} async-done(((f32[64,32,256]{2,1,0:T(8,128)}), f32[64,32,256]{2,1,0:T(8,128)}, u32[]{:S(2)}, u32[]{:S(2)}) %all-to-all-start) | async-done | bytes 2097184 | tf_op jit(solution)/shard_map/all_to_all | solution.py:45
  335.9 1.7 reduce_sum.125
  337.7 21.0 %psum.7 = f32[32]{0:T(128)} all-reduce(f32[32]{0:T(128)S(1)} %multiply_reduce_fusion), channel_id=1, replica_groups=mesh['sp_0'=8,'sp_1'=8,'tp'=8] {'tp'}, use_global_device_ids=true, to_apply=%region_17.18 | all-reduce | flops 32 | bytes 256 | tf_op jit(solution)/shard_map/psum | solution.py:131
  (272 shorter events, 121.1 us)
Async XLA Ops:
  7.2 3.6 copy-start
  7.2 48.3 %all-gather.13.cloned.1.call-start = ((), (), s32[]{:S(2)}) async-start(), calls=%async_computation.4 | async-start | bytes 1179648 | tf_op jit(solution)/shard_map/all_gather | solution.py:27
  10.8 2.1 copy-start.7
  12.8 2.4 copy-start.8
  13.9 83.4 %all-gather.11.cloned.1.call-start = ((), (), s32[]{:S(2)}) async-start(), calls=%async_computation.3 | async-start | bytes 1179648 | tf_op jit(solution)/shard_map/all_gather | solution.py:27
  15.2 44.1 %copy-start.10 = (f32[512,4]{0,1:T(4,128)S(1)}, f32[512,4]{0,1:T(4,128)}, u32[]{:S(2)}) copy-start(f32[512,4]{0,1:T(4,128)} %param.14) | copy-start | bytes 24580
  16.3 124.2 %all-gather.9.cloned.1.call-start = ((), (), s32[]{:S(2)}) async-start(), calls=%async_computation.2 | async-start | bytes 1179648 | tf_op jit(solution)/shard_map/all_gather | solution.py:27
  57.6 128.7 %all-gather.7.cloned.1.call-start = ((), (), s32[]{:S(2)}) async-start(), calls=%async_computation.1 | async-start | bytes 1179648 | tf_op jit(solution)/shard_map/all_gather | solution.py:27
  57.8 0.8 copy-start.1
  61.4 79.2 %copy-start.11 = (f32[4]{0:T(128)S(1)}, f32[4]{0:T(128)}, u32[]{:S(2)}) copy-start(f32[4]{0:T(128)} %get-tuple-element.1261) | copy-start | bytes 52
  62.9 79.6 %copy-start.5 = (f32[4,128,1,4]{3,1,2,0:T(8,128)S(1)}, f32[4,128,1,4]{3,1,2,0:T(8,128)}, u32[]{:S(2)}) copy-start(f32[4,128,1,4]{3,1,2,0:T(8,128)} %copy.214) | copy-start | bytes 24580
  62.9 79.6 %copy-start.6 = (f32[4,128,1,4]{3,1,2,0:T(8,128)S(1)}, f32[4,128,1,4]{3,1,2,0:T(8,128)}, u32[]{:S(2)}) copy-start(f32[4,128,1,4]{3,1,2,0:T(8,128)} %copy.217) | copy-start | bytes 24580
  196.1 13.5 %copy-start.3 = (bf16[4,128,1,4,64]{1,4,3,2,0:T(8,128)(2,1)S(1)}, bf16[4,128,1,4,64]{1,4,3,2,0:T(8,128)(2,1)}, u32[]{:S(2)}) copy-start(bf16[4,128,1,4,64]{1,4,3,2,0:T(8,128)(2,1)} %get-tuple-element.1807) | copy-start | bytes 786436 | tf_op jit(solution)/shard_map/transpose(jvp())/while
  210.0 1.0 copy-start.4
  217.3 13.5 %copy-start.3 = (bf16[4,128,1,4,64]{1,4,3,2,0:T(8,128)(2,1)S(1)}, bf16[4,128,1,4,64]{1,4,3,2,0:T(8,128)(2,1)}, u32[]{:S(2)}) copy-start(bf16[4,128,1,4,64]{1,4,3,2,0:T(8,128)(2,1)} %get-tuple-element.1807) | copy-start | bytes 786436 | tf_op jit(solution)/shard_map/transpose(jvp())/while
  231.2 1.0 copy-start.4
  238.5 13.5 %copy-start.3 = (bf16[4,128,1,4,64]{1,4,3,2,0:T(8,128)(2,1)S(1)}, bf16[4,128,1,4,64]{1,4,3,2,0:T(8,128)(2,1)}, u32[]{:S(2)}) copy-start(bf16[4,128,1,4,64]{1,4,3,2,0:T(8,128)(2,1)} %get-tuple-element.1807) | copy-start | bytes 786436 | tf_op jit(solution)/shard_map/transpose(jvp())/while
  252.4 0.9 copy-start.4
  259.7 13.5 %copy-start.3 = (bf16[4,128,1,4,64]{1,4,3,2,0:T(8,128)(2,1)S(1)}, bf16[4,128,1,4,64]{1,4,3,2,0:T(8,128)(2,1)}, u32[]{:S(2)}) copy-start(bf16[4,128,1,4,64]{1,4,3,2,0:T(8,128)(2,1)} %get-tuple-element.1807) | copy-start | bytes 786436 | tf_op jit(solution)/shard_map/transpose(jvp())/while
  273.5 0.9 copy-start.4
  280.6 10.7 %copy-start.2 = (f32[4,128,1,4]{3,2,1,0:T(1,128)S(1)}, f32[4,128,1,4]{3,2,1,0:T(1,128)}, u32[]{:S(2)}) copy-start(f32[4,128,1,4]{3,2,1,0:T(1,128)} %get-tuple-element.779) | copy-start | bytes 24580
  280.6 55.3 %all-to-all-start = ((f32[64,32,256]{2,1,0:T(8,128)}), f32[64,32,256]{2,1,0:T(8,128)}, u32[]{:S(2)}, u32[]{:S(2)}) async-start(f32[64,32,256]{2,1,0:T(8,128)} %bitcast.853), calls=%async_computation | async-start | bytes 4194304 | tf_op jit(solution)/shard_map/all_to_all | solution.py:45
  337.6 21.1 %copy-start.9 = (f32[32,256]{1,0:T(8,128)}, f32[32,256]{1,0:T(8,128)S(1)}, u32[]{:S(2)}) copy-start(f32[32,256]{1,0:T(8,128)S(1)} %reduce_sum.125) | copy-start | bytes 98308
Sparse Core Ops, SparseCore 0:
  14.0 41.3 all-gather.12
  57.6 39.7 all-gather.10
  99.4 41.0 all-gather.8
  142.5 39.9 all-gather.6
where the time goes:
time: 368 us; the launch traced here: 365 us
  waiting for transfers between devices  118 us (32%)
  blocking collectives  59.4 us (16%)
  matrix products  59 us (16%)
  local copies, waits for them, and re-layouts  58.2 us (16%)
  other arithmetic  45.6 us (12%)
  between operations  14.1 us (4%)
  starting transfers between devices  10.8 us (3%)
    all_gather x4, waiting for transfers between devices, prefix_by_axis(): pieces = jax.tree.map(lambda part: lax.all_gather(part, axis), subtotal)  73.8 us
    all_to_all x1, waiting for transfers between devices, summed_on_arrival(): blocks = lax.all_to_all(in_blocks(array, dim, size), axis, 0, 0, tiled=True)  43.9 us
    all_gather x3, blocking collectives, prefix_by_axis(): pieces = jax.tree.map(lambda part: lax.all_gather(part, axis), subtotal)  38.4 us
    dynamic_slice x32, local copies, waits for them, and re-layouts, local_pass(): final, outputs = lax.scan(block_step, state_in, pieces)  23.1 us
    psum x1, blocking collectives, on_device(): row_norms = lax.psum(jnp.sum(weight_grad * weight_grad, axis=1), 'tp')  21 us
    dot_general x12, matrix products, block_step(): jnp.einsum('rgn,rgjp->gjpn', key_rows, values * to_end[..., None], precis...  17.6 us
    dot_general x12, matrix products, block_step(): scores = jnp.einsum('sgn,rgn->srg', queries, key_rows, precision=exact_mode)  14.8 us
    dynamic_update_slice x28, local copies, waits for them, and re-layouts, local_pass(): final, outputs = lax.scan(block_step, state_in, pieces)  12.7 us
  transfers between devices with their start and end apart: 5, of which 4 were waited for; matrix products, arithmetic and copies ran while one was open for 17% of the time, Pallas kernels for 0%

commit v1 on v0

v1 whole, which is shorter than its diff:
```python
import functools

import jax
import jax.numpy as jnp
from jax import lax
from jax.experimental import pallas as pl
from jax.experimental.pallas import tpu as pltpu
from jax.sharding import Mesh
from jax.sharding import PartitionSpec as P

SP = ("sp_0", "sp_1")
F32 = jnp.float32
BF16 = jnp.bfloat16
MESH = pl.DeviceIdType.MESH
LOADS = 4
CHUNKS = 4
ORDER = (2, 1, 3, 0)


def dot(a, b, a_dim, b_dim):
    return lax.dot_general(a, b, (((a_dim,), (b_dim,)), ((), ())), preferred_element_type=F32)


def thirds(x):
    high = x.astype(BF16)
    rest = x - high.astype(F32)
    middle = rest.astype(BF16)
    low = (rest - middle.astype(F32)).astype(BF16)
    return high, middle, low


def far_first(n):
    return sorted(range(n), key=lambda d: -min(d, n - d))


def kernel(
    nz, ny, nt,
    decay_hbm, grad_hbm, query_hbm, key_hbm, input_hbm, weight_hbm,
    query_grad, key_grad, decay_grad, weight_grad, norms,
    decay, grad, query, key, block_in, weight,
    value, value_of, grad_of, rise, fall, grad_rise, value_fall, tri, down, across,
    send_b, recv_b, out_b, in_b, send_f, recv_f, out_f, in_f,
    own_state, state_grad, values_grad, mixed, local_q, local_k, rounded,
    turned_a, turned_b, partial_a, partial_b, ring_ap, ring_am, ring_bp, ring_bm,
    block_a, block_b, last_a, last_b, norm_out, norm_in,
    load_sem, scan_send, scan_recv, ring_send, ring_recv, last_send, last_recv, norm_send, norm_recv,
):
    z, y, t = lax.axis_index("sp_0"), lax.axis_index("sp_1"), lax.axis_index("tp")
    shards = nz * ny
    me = z * ny + y
    rows, width = grad.shape
    heads = decay.shape[0]
    depth = width // heads
    pair = 2 * depth
    state = query.shape[1]
    piece = rows // LOADS

    loads = [
        pltpu.make_async_copy(decay_hbm, decay, load_sem.at[0]),
        pltpu.make_async_copy(grad_hbm, grad, load_sem.at[1]),
        pltpu.make_async_copy(query_hbm, query, load_sem.at[2]),
        pltpu.make_async_copy(weight_hbm, weight, load_sem.at[3]),
        pltpu.make_async_copy(key_hbm, key, load_sem.at[4]),
    ]
    for i in range(LOADS):
        part = pl.ds(i * piece, piece)
        loads.append(pltpu.make_async_copy(input_hbm.at[part], block_in.at[part], load_sem.at[5 + i]))
    for copy in loads:
        copy.start()

    barrier = pltpu.get_barrier_semaphore()

    def greet(i, carry):
        other = lax.rem(me + i, shards)
        pl.semaphore_signal(
            barrier, inc=1, device_id={"sp_0": lax.div(other, ny), "sp_1": lax.rem(other, ny)}, device_id_type=MESH
        )
        return carry

    lax.fori_loop(1, shards, greet, 0)
    for j in range(1, nt):
        pl.semaphore_signal(barrier, inc=1, device_id={"tp": lax.rem(t + j, nt)}, device_id_type=MESH)

    def exchange(source, target, number):
        def one(dz, dy):
            oz, oy = lax.rem(z + dz, nz), lax.rem(y + dy, ny)
            pltpu.make_async_remote_copy(
                src_ref=source.at[oz * ny + oy], dst_ref=target.at[me],
                send_sem=scan_send.at[number], recv_sem=scan_recv.at[number],
                device_id={"sp_0": oz, "sp_1": oy}, device_id_type=MESH,
            ).start()

        def plane(i, carry):
            for dy in far_first(ny):
                one(1 + lax.rem(i + nz // 2 - 1, nz - 1), dy)
            return carry

        lax.fori_loop(0, nz - 1, plane, 0)
        for dy in far_first(ny):
            if dy:
                one(0, dy)
        target[me] = source[me]

    def arrived(buffer, sem):
        pltpu.make_async_copy(buffer, buffer, sem).wait()

    early = lax.broadcasted_iota(jnp.int32, (rows, rows), 0) <= lax.broadcasted_iota(jnp.int32, (rows, rows), 1)
    tri[...] = jnp.where(early, 1.0, 0.0).astype(BF16)

    def stacked(x):
        high, middle, low = thirds(x)
        return jnp.concatenate(
            [high.astype(F32), middle.astype(F32), low.astype(F32), jnp.zeros_like(x)], axis=0
        ).astype(BF16)

    def unstacked(x):
        return x[0:8] + x[8:16] + x[16:24]

    loads[0].wait()
    log8 = jnp.concatenate([decay[...]] * (8 // heads), axis=0)
    across[...] = unstacked(dot(stacked(log8), tri[...], 1, 0))
    down[...] = jnp.concatenate([across[...]] * 16, axis=0).T
    lane = lax.broadcasted_iota(jnp.int32, (rows, pair), 1)
    for h in range(0, heads, 2):
        cols = pl.ds(h * depth, pair)
        cum = jnp.where(
            lane < depth,
            jnp.broadcast_to(down[:, h : h + 1], (rows, pair)),
            jnp.broadcast_to(down[:, h + 1 : h + 2], (rows, pair)),
        )
        rise[:, cols] = jnp.exp(cum)
        fall[:, cols] = jnp.exp(cum[rows - 1 : rows, :] - cum)

    loads[1].wait()
    loads[2].wait()
    grad_rise[...] = (grad[...].astype(F32) * rise[...]).astype(BF16)
    own = dot(grad_rise[...], query[...], 0, 0)
    for h in range(heads):
        send_b[:, h, :] = own[h * depth : (h + 1) * depth, :]
    send_b[:, heads, :] = jnp.broadcast_to(down[rows - 1 : rows, :], (shards, state))
    pl.semaphore_wait(barrier, shards - 1 + nt - 1)
    exchange(send_b, recv_b, 0)

    loads[3].wait()
    for i in range(LOADS):
        loads[5 + i].wait()
        part = pl.ds(i * piece, piece)
        value[part, :] = dot(block_in[part, :], weight[...], 1, 0).astype(BF16)
    loads[4].wait()
    value_fall[...] = (value[...].astype(F32) * fall[...]).astype(BF16)
    own_state[...] = dot(value_fall[...], key[...], 0, 0)
    for h in range(heads):
        send_f[:, h, :] = own_state[h * depth : (h + 1) * depth, :]
    exchange(send_f, recv_f, 1)

    tall_a, tall_b = turned_a.shape[1], turned_b.shape[1]
    small = tall_a // ny
    for i in range(nz):
        turned_a[i] = block_in[:, i * tall_a : (i + 1) * tall_a].T
    for i in range(nz):
        for j in range(ny):
            turned_b[j, i * small : (i + 1) * small, :] = turned_a[i, j * small : (j + 1) * small, :]
    for h in range(heads):
        cols = pl.ds((h // 2) * pair, pair)
        mine = (lane < depth) if h % 2 == 0 else (lane >= depth)
        grad_of[h] = jnp.where(mine, grad[:, cols].astype(F32), 0.0).astype(BF16)
        value_of[h] = jnp.where(mine, value[:, cols].astype(F32), 0.0).astype(BF16)

    def first(buffer):
        return buffer.at[pl.ds(0, shards - 1)]

    arrived(first(recv_b), scan_recv.at[0])
    logs = recv_b[:, heads, :]
    logs = jnp.concatenate([logs] * (128 // shards), axis=0).T
    factors = jnp.exp(logs[0:heads, :])

    def factor(k):
        return jnp.broadcast_to(factors[:, k : k + 1], (heads, state))

    total = jnp.zeros((heads, state), F32)
    for k in reversed(range(shards)):
        out_b[k] = total
        if k:
            total = factor(k) * total + recv_b[k, 0:heads, :]
    exchange(out_b, in_b, 2)

    arrived(first(recv_f), scan_recv.at[1])
    total = jnp.zeros((heads, state), F32)
    for k in range(shards):
        out_f[k] = total
        if k < shards - 1:
            total = factor(k) * total + recv_f[k]
    exchange(out_f, in_f, 3)

    half = rows // 2
    causal = lax.broadcasted_iota(jnp.int32, (half, half), 0) >= lax.broadcasted_iota(jnp.int32, (half, half), 1)
    for late, early_block in ((0, 0), (1, 0), (1, 1)):
        to, of = pl.ds(late * half, half), pl.ds(early_block * half, half)
        scores = dot(query[to, :], key[of, :], 1, 1)
        score_grad = jnp.zeros((half, half), F32)
        for h0 in range(0, heads, 2):
            cols = pl.ds(h0 * depth, pair)
            for h in (h0, h0 + 1):
                gap = jnp.broadcast_to(down[to, h : h + 1], (half, half)) - jnp.broadcast_to(
                    across[h : h + 1, of], (half, half)
                )
                decayed = jnp.exp(jnp.minimum(gap, 0.0))
                if late == early_block:
                    decayed = jnp.where(causal, decayed, 0.0)
                score_grad += dot(grad_of[h, to, :], value[of, cols], 1, 1) * decayed
                weighted = (scores * decayed).astype(BF16)
                to_value = dot(weighted, grad_of[h, to, :], 0, 0)
                to_mixed = dot(weighted, value_of[h, of, :], 1, 0)
                if h == h0 and late == early_block:
                    if late == 0:
                        values_grad[of, cols] = to_value
                    else:
                        values_grad[of, cols] = to_value
                else:
                    values_grad[of, cols] += to_value
                if h == h0 and early_block == 0:
                    mixed[to, cols] = to_mixed
                else:
                    mixed[to, cols] += to_mixed
        score_grad = score_grad.astype(BF16)
        to_q = dot(score_grad, key[of, :], 1, 0)
        to_k = dot(score_grad, query[to, :], 0, 0)
        if early_block == 0:
            local_q[to, :] = to_q
        else:
            local_q[to, :] += to_q
        if late == early_block:
            local_k[of, :] = to_k
        else:
            local_k[of, :] += to_k

    arrived(first(in_b), scan_recv.at[2])
    for h in range(heads):
        state_grad[h * depth : (h + 1) * depth, :] = in_b[:, h, :]
    state_grad_16 = state_grad[...].astype(BF16)
    values_grad[...] += fall[...] * dot(key[...], state_grad_16, 1, 1)
    rounded[...] = values_grad[...].astype(BF16)

    axes = (
        ("sp_0", nz, z, "sp_1", ny, y, turned_a, partial_a, (ring_ap, ring_am), block_a, last_a),
        ("sp_1", ny, y, "sp_0", nz, z, turned_b, partial_b, (ring_bp, ring_bm), block_b, last_b),
    )
    reach = ring_ap.shape[0]

    def product(a, r):
        _, n, at, _, n_o, at_o, turned, partial, _, _, _ = axes[a]
        block = dot(turned[lax.rem(at + r, n)], rounded[:, a * pair : (a + 1) * pair], 1, 0)
        for q in range(n_o):
            where = pl.multiple_of(lax.rem(q + n_o - at_o, n_o) * small, small)
            partial[r, pl.ds(where, small), :] = block[q * small : (q + 1) * small, :]

    def comes(way, s, c):
        return s > 0 or (c < CHUNKS // 2) == (way == 0)

    def slot(a, way, s, c):
        return ((a * 2 + way) * reach + s) * CHUNKS + c

    def span(a, c):
        tall = axes[a][7].shape[1] // CHUNKS
        return pl.ds(c * tall, tall)

    def block_of(a, way, s):
        n = axes[a][1]
        return reach - s if way == 0 else n - reach + s

    def hop(a, way, s, c):
        name, n, at, _, _, _, _, partial, ring, _, _ = axes[a]
        pltpu.make_async_remote_copy(
            src_ref=partial.at[block_of(a, way, s), span(a, c)], dst_ref=ring[way].at[s, span(a, c)],
            send_sem=ring_send.at[a], recv_sem=ring_recv.at[slot(a, way, s, c)],
            device_id={name: lax.rem(at + (1 if way == 0 else n - 1), n)}, device_id_type=MESH,
        ).start()

    def landed(a, way, s, c):
        arrived(axes[a][8][way].at[s, span(a, c)], ring_recv.at[slot(a, way, s, c)])
        return axes[a][8][way][s, span(a, c), :]

    def finish_queries():
        arrived(first(in_f), scan_recv.at[3])
        before = jnp.concatenate([in_f[:, h, :] for h in range(heads)], axis=0)
        query_grad[...] = local_q[...] + dot(grad_rise[...], before.astype(BF16), 1, 0)

    def finish_keys():
        key_grad[...] = local_k[...] + dot(value_fall[...], state_grad[...].astype(BF16), 1, 0)

    def finish_decays():
        before = jnp.concatenate([in_f[:, h, :] for h in range(heads)], axis=0)
        whole = mixed[...] + rise[...] * dot(query[...], before.astype(BF16), 1, 1)
        change = grad[...].astype(F32) * whole - value[...].astype(F32) * values_grad[...]
        owner = lax.broadcasted_iota(jnp.int32, (8, width), 1) // depth
        pick = jnp.where(owner == lax.broadcasted_iota(jnp.int32, (8, width), 0), 1.0, 0.0).astype(BF16)
        by_head = sum(dot(pick, part, 1, 1) for part in thirds(change))
        through = unstacked(dot(stacked(by_head), tri[...], 1, 1))
        row = lax.broadcasted_iota(jnp.int32, (8, 1), 0)
        beyond = jnp.zeros((8, 1), F32)
        for h in range(heads):
            part = slice(h * depth, (h + 1) * depth)
            end = before[part] * jnp.exp(down[rows - 1 : rows, h : h + 1]) + own_state[part, :]
            flow = jnp.sum(jnp.sum(end * state_grad[part, :], axis=0, keepdims=True), axis=1, keepdims=True)
            beyond = jnp.where(row == h, flow, beyond)
        decay_grad[...] = (through + beyond)[0:heads, :]

    extra = [finish_queries, finish_keys, finish_decays]
    for a in range(2):
        product(a, reach)
    for c in ORDER:
        for a in range(2):
            for way in range(2):
                if comes(way, 0, c):
                    hop(a, way, 0, c)
    for s in range(1, reach):
        for a in range(2):
            for way in range(2):
                product(a, block_of(a, way, s))
        if s > 1 and extra:
            extra.pop(0)()
        for c in ORDER:
            for a in range(2):
                for way in range(2):
                    if comes(way, s - 1, c):
                        axes[a][7][block_of(a, way, s), span(a, c), :] += landed(a, way, s - 1, c)
                    hop(a, way, s, c)
    for a in range(2):
        product(a, 0)
    for c in ORDER:
        for a in range(2):
            _, _, _, name_o, n_o, at_o, _, partial, _, block, last = axes[a]
            block[span(a, c), :] = partial[0, span(a, c), :] + landed(a, 0, reach - 1, c) + landed(a, 1, reach - 1, c)
            each = n_o // CHUNKS
            for j in range(c * each, (c + 1) * each):
                part = pl.ds(j * small, small)
                if j == 0:
                    last[0] = block[part, :]
                else:
                    pltpu.make_async_remote_copy(
                        src_ref=block.at[part], dst_ref=last.at[j], send_sem=last_send.at[a], recv_sem=last_recv.at[a],
                        device_id={name_o: lax.rem(at_o + j, n_o)}, device_id_type=MESH,
                    ).start()
    for work in extra:
        work()

    squares = jnp.zeros((small, pair), F32)
    for a in range(2):
        n_o, last = axes[a][4], axes[a][10]
        arrived(last.at[pl.ds(1, n_o - 1)], last_recv.at[a])
        done = last[0]
        for j in range(1, n_o):
            done += last[j]
        weight_grad[:, a * pair : (a + 1) * pair] = done
        squares += done * done
    ones = jnp.ones((8, pair), BF16)
    own_norms = sum(dot(ones, part, 1, 1) for part in thirds(squares))
    norm_out[...] = jnp.zeros_like(norm_out)
    norm_out[:, 0:small] = own_norms
    for j in range(1, nt):
        pltpu.make_async_remote_copy(
            src_ref=norm_out, dst_ref=norm_in.at[j], send_sem=norm_send, recv_sem=norm_recv,
            device_id={"tp": lax.rem(t + j, nt)}, device_id_type=MESH,
        ).start()
    if nt > 1:
        arrived(norm_in.at[pl.ds(1, nt - 1)], norm_recv)
    sums = norm_out[...]
    for j in range(1, nt):
        sums += norm_in[j]
    norms[...] = sums[0:1, 0:small]

    for i, buffer in enumerate((send_b, send_f, out_b, out_f)):
        arrived(first(buffer), scan_send.at[i])
    for a in range(2):
        n, n_o, partial, last = axes[a][1], axes[a][4], axes[a][7], axes[a][10]
        arrived(partial.at[pl.ds(0, n - 1)], ring_send.at[a])
        arrived(last.at[pl.ds(1, n_o - 1)], last_send.at[a])
    if nt > 1:
        arrived(norm_in.at[pl.ds(1, nt - 1)], norm_send)


def on_device(nz, ny, nt, block_input, value_weight, queries, key_rows, log_decay, out_grad):
    rows, model = block_input.shape
    width, heads, state = out_grad.shape[1], log_decay.shape[1], queries.shape[1]
    shards = nz * ny
    pair = 2 * (width // heads)
    reach = nz // 2
    tall_a, tall_b, small = model // nz, model // ny, model // shards
    vmem, dma = pltpu.VMEM, pltpu.SemaphoreType.DMA
    shape = jax.ShapeDtypeStruct
    scratch = [
        vmem((heads, rows), F32), vmem((rows, width), BF16), vmem((rows, state), BF16), vmem((rows, state), BF16),
        vmem((rows, model), BF16), vmem((model, width), BF16),
        vmem((rows, width), BF16), vmem((heads, rows, pair), BF16), vmem((heads, rows, pair), BF16),
        vmem((rows, width), F32), vmem((rows, width), F32), vmem((rows, width), BF16), vmem((rows, width), BF16),
        vmem((rows, rows), BF16), vmem((rows, 128), F32), vmem((8, rows), F32),
        vmem((shards, 8, state), F32), vmem((shards, 8, state), F32), vmem((shards, heads, state), F32), vmem((shards, heads, state), F32),
        vmem((shards, heads, state), F32), vmem((shards, heads, state), F32), vmem((shards, heads, state), F32), vmem((shards, heads, state), F32),
        vmem((width, state), F32), vmem((width, state), F32), vmem((rows, width), F32), vmem((rows, width), F32),
        vmem((rows, state), F32), vmem((rows, state), F32), vmem((rows, width), BF16),
        vmem((nz, tall_a, rows), BF16), vmem((ny, tall_b, rows), BF16), vmem((nz, tall_a, pair), F32), vmem((ny, tall_b, pair), F32),
        vmem((reach, tall_a, pair), F32), vmem((reach, tall_a, pair), F32), vmem((reach, tall_b, pair), F32), vmem((reach, tall_b, pair), F32),
        vmem((tall_a, pair), F32), vmem((tall_b, pair), F32), vmem((ny, small, pair), F32), vmem((nz, small, pair), F32),
        vmem((8, 128), F32), vmem((nt, 8, 128), F32),
        dma((5 + LOADS,)), dma((4,)), dma((4,)), dma((2,)), dma((4 * reach * CHUNKS,)), dma((2,)), dma((2,)), dma, dma,
    ]
    query_grad, key_grad, decay_grad, weight_grad, norms = pl.pallas_call(
        functools.partial(kernel, nz, ny, nt),
        out_shape=(
            shape((rows, state), F32), shape((rows, state), F32), shape((heads, rows), F32),
            shape((small, width), F32), shape((1, small), F32),
        ),
        in_specs=[pl.BlockSpec(memory_space=pl.ANY)] * 6,
        out_specs=(pl.BlockSpec(memory_space=pltpu.VMEM),) * 5,
        scratch_shapes=scratch,
        compiler_params=pltpu.CompilerParams(
            collective_id=0, has_side_effects=True, vmem_limit_bytes=56 * 1024 * 1024
        ),
    )(log_decay.T, out_grad, queries, key_rows, block_input, value_weight)
    return query_grad, key_grad, decay_grad.T, weight_grad, norms.reshape(small)


def solution(mesh):
    nz = ny = 8
    nt = mesh.shape["tp"]
    split = Mesh(mesh.devices.reshape(nz, ny, nt), ("sp_0", "sp_1", "tp"))
    return jax.shard_map(
        functools.partial(on_device, nz, ny, nt),
        mesh=split,
        in_specs=(P(SP, None), P(None, "tp"), P(SP, "tp"), P(SP, "tp"), P(SP, "tp"), P(SP, "tp")),
        out_specs=(P(SP, "tp"), P(SP, "tp"), P(SP, "tp"), P(SP, "tp"), P(SP)),
        check_vma=False,
    )
```

time: 368 us -> 71.8 us (0.20)
  waiting for transfers between devices: 118 us -> 0 us
  Pallas kernels: 0 us -> 63.8 us
  blocking collectives: 59.4 us -> 0 us
  matrix products: 59 us -> 0 us
  local copies, waits for them, and re-layouts: 58.2 us -> 7.11 us
  other arithmetic: 45.6 us -> 0 us
  between operations: 14.1 us -> 0.64 us
  starting transfers between devices: 10.8 us -> 0 us
    all_gather x4 -> x0, waiting for transfers between devices: 73.8 us -> none  [prefix_by_axis(): pieces = jax.tree.map(lambda part: lax.all_gather(part, axis), subtotal)]
    pallas_call x0 -> x1, Pallas kernels: none -> 63.8 us  [on_device(): pl.pallas_call(functools.partial(kernel, nz, ny, nt), out_shape=(shape((r...]
    dot_general x48 -> x0, matrix products: 59 us -> none  [the longest x12 17.6 us: block_step(): jnp.einsum('rgn,rgjp->gjpn', key_rows, values * to_end[..., None], precis...]
    all_to_all x1 -> x0, waiting for transfers between devices: 43.9 us -> none  [summed_on_arrival(): blocks = lax.all_to_all(in_blocks(array, dim, size), axis, 0, 0, tiled=True)]
    all_gather x3 -> x0, blocking collectives: 38.4 us -> none  [prefix_by_axis(): pieces = jax.tree.map(lambda part: lax.all_gather(part, axis), subtotal)]
    dynamic_slice x32 -> x0, local copies, waits for them, and re-layouts: 23.1 us -> none  [local_pass(): final, outputs = lax.scan(block_step, state_in, pieces)]
    psum x1 -> x0, blocking collectives: 21 us -> none  [on_device(): row_norms = lax.psum(jnp.sum(weight_grad * weight_grad, axis=1), 'tp')]
    reduce_sum x14 -> x0, other arithmetic: 12.8 us -> none  [the longest x4 4.11 us: block_step(): new_memory = jnp.exp(cumulative[-1])[..., None, None] * memory + fresh_state]
  transfers between devices with their start and end apart: 5 -> 0, of which waited for: 4 -> 0; matrix products, arithmetic and copies ran while one was open for 17% -> 0% of each run, Pallas kernels for 0% -> 0%
where the time goes in v1:
time: 71.8 us; the launch traced here: 71.6 us
  Pallas kernels  63.8 us (89%)
  local copies, waits for them, and re-layouts  7.11 us (10%)
    pallas_call x1, Pallas kernels, on_device(): pl.pallas_call(functools.partial(kernel, nz, ny, nt), out_shape=(shape((r...  63.8 us
    unnamed x5, local copies, waits for them, and re-layouts  7.11 us

profile of v1, /device:TPU:1, one launch (start us, length us, event | category | flops | bytes accessed | tf_op | source)
XLA Modules:
  0.0 71.6 jit_solution(9206695125296726613)
XLA Ops:
  0.6 63.8 %shard_map.101 = (f32[512,128]{1,0:T(8,128)}, f32[512,128]{1,0:T(8,128)}, f32[4,512]{1,0:T(4,128)}, f32[32,256]{1,0:T(8,128)}, f32[1,32]{1,0:T(1,128)}) custom-call(f32[4,512]{1,0:T(4,128)} %bitcast.3, bf16[512,256]{1,0:T(8,128)(2,1)} %grad_hbm.1, bf16[512,128]{1,0:T(8,128)(2,1)} %query_hbm.1, bf16[512,128]{1,0:T(8,128)(2,1)} %key_hbm.1, ...), custom_call_target="tpu_custom_call" | custom-call | tf_op jit(solution)/shard_map/pallas_call | solution.py:407
  64.4 1.7 %copy.16 = f32[512,128]{1,0:T(8,128)} copy(f32[512,128]{1,0:T(8,128)} %get-tuple-element.20) | data formatting | bytes 524288
  66.1 1.7 %copy.17 = f32[512,128]{1,0:T(8,128)} copy(f32[512,128]{1,0:T(8,128)} %get-tuple-element.21) | data formatting | bytes 524288
  67.8 1.3 %copy.18 = f32[512,4]{0,1:T(4,128)} copy(f32[512,4]{0,1:T(4,128)} %bitcast.4) | data formatting | bytes 16384
  69.1 1.4 %copy.19 = f32[32,256]{1,0:T(8,128)} copy(f32[32,256]{1,0:T(8,128)} %get-tuple-element.23) | data formatting | bytes 65536
  70.4 1.1 %copy.20 = f32[32]{0:T(128)} copy(f32[32]{0:T(128)} %bitcast.5) | data formatting | bytes 256

commit v2 on v1

--- a/solution.py
+++ b/solution.py
@@ -13,8 +13,7 @@
 BF16 = jnp.bfloat16
 MESH = pl.DeviceIdType.MESH
 LOADS = 4
-CHUNKS = 4
-ORDER = (2, 1, 3, 0)
+CHUNKS = 8
 
 
 def dot(a, b, a_dim, b_dim):
@@ -33,17 +32,23 @@
     return sorted(range(n), key=lambda d: -min(d, n - d))
 
 
+def per_piece(n):
+    each = max(n // CHUNKS, 1)
+    seen = [d // each for d in far_first(n)]
+    return list(dict.fromkeys(seen))
+
+
 def kernel(
     nz, ny, nt,
     decay_hbm, grad_hbm, query_hbm, key_hbm, input_hbm, weight_hbm,
     query_grad, key_grad, decay_grad, weight_grad, norms,
     decay, grad, query, key, block_in, weight,
     value, value_of, grad_of, rise, fall, grad_rise, value_fall, tri, down, across,
-    send_b, recv_b, out_b, in_b, send_f, recv_f, out_f, in_f,
-    own_state, state_grad, values_grad, mixed, local_q, local_k, rounded,
+    logs, row_logs, scan_send_buf, scan_recv_buf, row_send, row_recv, scan_out, scan_in, beyond_rows,
+    own_state, state_grad, before, values_grad, mixed, local_q, local_k, rounded,
     turned_a, turned_b, partial_a, partial_b, ring_ap, ring_am, ring_bp, ring_bm,
     block_a, block_b, last_a, last_b, norm_out, norm_in,
-    load_sem, scan_send, scan_recv, ring_send, ring_recv, last_send, last_recv, norm_send, norm_recv,
+    load_sem, log_send, log_recv, row_send_sem, row_recv_sem, scan_send, scan_recv, ring_send, ring_recv, last_send, last_recv, norm_send, norm_recv,
 ):
     z, y, t = lax.axis_index("sp_0"), lax.axis_index("sp_1"), lax.axis_index("tp")
     shards = nz * ny
@@ -70,39 +75,28 @@
 
     barrier = pltpu.get_barrier_semaphore()
 
-    def greet(i, carry):
-        other = lax.rem(me + i, shards)
-        pl.semaphore_signal(
-            barrier, inc=1, device_id={"sp_0": lax.div(other, ny), "sp_1": lax.rem(other, ny)}, device_id_type=MESH
-        )
-        return carry
-
-    lax.fori_loop(1, shards, greet, 0)
-    for j in range(1, nt):
-        pl.semaphore_signal(barrier, inc=1, device_id={"tp": lax.rem(t + j, nt)}, device_id_type=MESH)
-
-    def exchange(source, target, number):
-        def one(dz, dy):
-            oz, oy = lax.rem(z + dz, nz), lax.rem(y + dy, ny)
+    lines = {"sp_0": (z, nz), "sp_1": (y, ny), "tp": (t, nt)}
+
+    def others(name):
+        at, n = lines[name]
+        return [lax.rem(at + d, n) for d in far_first(n) if d]
+
+    for name in lines:
+        for other in others(name):
+            pl.semaphore_signal(barrier, inc=1, device_id={name: other}, device_id_type=MESH)
+
+    def along(name, source, target, send_sem, recv_sem):
+        for other in others(name):
             pltpu.make_async_remote_copy(
-                src_ref=source.at[oz * ny + oy], dst_ref=target.at[me],
-                send_sem=scan_send.at[number], recv_sem=scan_recv.at[number],
-                device_id={"sp_0": oz, "sp_1": oy}, device_id_type=MESH,
+                src_ref=source(other), dst_ref=target, send_sem=send_sem, recv_sem=recv_sem,
+                device_id={name: other}, device_id_type=MESH,
             ).start()
-
-        def plane(i, carry):
-            for dy in far_first(ny):
-                one(1 + lax.rem(i + nz // 2 - 1, nz - 1), dy)
-            return carry
-
-        lax.fori_loop(0, nz - 1, plane, 0)
-        for dy in far_first(ny):
-            if dy:
-                one(0, dy)
-        target[me] = source[me]
 
     def arrived(buffer, sem):
         pltpu.make_async_copy(buffer, buffer, sem).wait()
+
+    def all_but_one(buffer):
+        return buffer.at[pl.ds(0, buffer.shape[0] - 1)]
 
     early = lax.broadcasted_iota(jnp.int32, (rows, rows), 0) <= lax.broadcasted_iota(jnp.int32, (rows, rows), 1)
     tri[...] = jnp.where(early, 1.0, 0.0).astype(BF16)
@@ -134,12 +128,27 @@
     loads[1].wait()
     loads[2].wait()
     grad_rise[...] = (grad[...].astype(F32) * rise[...]).astype(BF16)
-    own = dot(grad_rise[...], query[...], 0, 0)
-    for h in range(heads):
-        send_b[:, h, :] = own[h * depth : (h + 1) * depth, :]
-    send_b[:, heads, :] = jnp.broadcast_to(down[rows - 1 : rows, :], (shards, state))
-    pl.semaphore_wait(barrier, shards - 1 + nt - 1)
-    exchange(send_b, recv_b, 0)
+    tiles = depth // ny
+
+    def pack(number, own):
+        for g in range(ny):
+            for h in range(heads):
+                at = h * depth + g * tiles
+                scan_send_buf[number, g, h] = own[at : at + tiles, :]
+
+    pack(0, dot(grad_rise[...], query[...], 0, 0))
+    logs[y] = down[rows - 1 : rows, :]
+
+    def first_round(number):
+        along(
+            "sp_1", lambda other: scan_send_buf.at[number, other], scan_recv_buf.at[number, y],
+            scan_send.at[number, 0], scan_recv.at[number, 0],
+        )
+        scan_recv_buf[number, y] = scan_send_buf[number, y]
+
+    pl.semaphore_wait(barrier, nz - 1 + ny - 1 + nt - 1)
+    along("sp_1", lambda other: logs.at[y], logs.at[y], log_send.at[0], log_recv.at[0])
+    first_round(0)
 
     loads[3].wait()
     for i in range(LOADS):
@@ -149,9 +158,8 @@
     loads[4].wait()
     value_fall[...] = (value[...].astype(F32) * fall[...]).astype(BF16)
     own_state[...] = dot(value_fall[...], key[...], 0, 0)
-    for h in range(heads):
-        send_f[:, h, :] = own_state[h * depth : (h + 1) * depth, :]
-    exchange(send_f, recv_f, 1)
+    pack(1, own_state[...])
+    first_round(1)
 
     tall_a, tall_b = turned_a.shape[1], turned_b.shape[1]
     small = tall_a // ny
@@ -165,32 +173,6 @@
         mine = (lane < depth) if h % 2 == 0 else (lane >= depth)
         grad_of[h] = jnp.where(mine, grad[:, cols].astype(F32), 0.0).astype(BF16)
         value_of[h] = jnp.where(mine, value[:, cols].astype(F32), 0.0).astype(BF16)
-
-    def first(buffer):
-        return buffer.at[pl.ds(0, shards - 1)]
-
-    arrived(first(recv_b), scan_recv.at[0])
-    logs = recv_b[:, heads, :]
-    logs = jnp.concatenate([logs] * (128 // shards), axis=0).T
-    factors = jnp.exp(logs[0:heads, :])
-
-    def factor(k):
-        return jnp.broadcast_to(factors[:, k : k + 1], (heads, state))
-
-    total = jnp.zeros((heads, state), F32)
-    for k in reversed(range(shards)):
-        out_b[k] = total
-        if k:
-            total = factor(k) * total + recv_b[k, 0:heads, :]
-    exchange(out_b, in_b, 2)
-
-    arrived(first(recv_f), scan_recv.at[1])
-    total = jnp.zeros((heads, state), F32)
-    for k in range(shards):
-        out_f[k] = total
-        if k < shards - 1:
-            total = factor(k) * total + recv_f[k]
-    exchange(out_f, in_f, 3)
 
     half = rows // 2
     causal = lax.broadcasted_iota(jnp.int32, (half, half), 0) >= lax.broadcasted_iota(jnp.int32, (half, half), 1)
@@ -234,9 +216,86 @@
         else:
             local_k[of, :] += to_k
 
-    arrived(first(in_b), scan_recv.at[2])
-    for h in range(heads):
-        state_grad[h * depth : (h + 1) * depth, :] = in_b[:, h, :]
+    arrived(all_but_one(logs), log_recv.at[0])
+    line_logs = [logs[k] for k in range(ny)]
+    row_logs[z] = sum(line_logs[1:], line_logs[0])
+    along("sp_0", lambda other: row_logs.at[z], row_logs.at[z], log_send.at[1], log_recv.at[1])
+
+    def splat(row):
+        return [jnp.broadcast_to(row[:, h : h + 1], (tiles, state)) for h in range(heads)]
+
+    factors = [splat(jnp.exp(row)) for row in line_logs]
+
+    def steps(number, n):
+        return list(range(n)) if number else list(reversed(range(n)))
+
+    def row_copy(number, to, slot, sem):
+        return pltpu.make_async_remote_copy(
+            src_ref=row_send.at[number], dst_ref=row_recv.at[number, slot],
+            send_sem=row_send_sem.at[number, sem], recv_sem=row_recv_sem.at[number, slot],
+            device_id={"sp_0": to}, device_id_type=MESH,
+        )
+
+    def each_row(number, sent, sem):
+        for k in range(nz):
+
+            @pl.when(k > z if bool(number) == sent else k < z)
+            def _():
+                arrived(row_recv.at[number, k], sem.at[number, k])
+
+    def line(number):
+        arrived(all_but_one(scan_recv_buf.at[number]), scan_recv.at[number, 0])
+        total = [jnp.zeros((tiles, state), F32) for _ in range(heads)]
+        for k in steps(number, ny):
+            for h in range(heads):
+                scan_out[number, k, h] = total[h]
+                total[h] = factors[k][h] * total[h] + scan_recv_buf[number, k, h]
+        for h in range(heads):
+            row_send[number, h] = total[h]
+        for d in range(1, nz):
+            other = z + d if number else z - d
+            inside = other < nz if number else other >= 0
+
+            @pl.when(inside)
+            def _():
+                row_copy(number, other, z, other).start()
+
+    def line_factors(k):
+        return splat(jnp.exp(row_logs[k]))
+
+    def plane(number):
+        each_row(number, False, row_recv_sem)
+        total = [jnp.zeros((tiles, state), F32) for _ in range(heads)]
+        for k in steps(number, nz):
+            for h in range(heads):
+                beyond_rows[k, h] = total[h]
+                total[h] = whole_factors[k][h] * total[h] + row_recv[number, k, h]
+        reaching = [beyond_rows[z, h] for h in range(heads)]
+        for k in steps(number, ny):
+            for h in range(heads):
+                scan_out[number, k, h] += reaching[h]
+                reaching[h] = factors[k][h] * reaching[h]
+        scan_in[number, y] = scan_out[number, y]
+        along(
+            "sp_1", lambda other: scan_out.at[number, other], scan_in.at[number, y],
+            scan_send.at[number, 2], scan_recv.at[number, 2],
+        )
+
+    def unpack(number, target):
+        arrived(all_but_one(scan_in.at[number]), scan_recv.at[number, 2])
+        for g in range(ny):
+            for h in range(heads):
+                at = h * depth + g * tiles
+                target[at : at + tiles, :] = scan_in[number, g, h]
+
+    line(0)
+    arrived(all_but_one(row_logs), log_recv.at[1])
+    whole_factors = [line_factors(k) for k in range(nz)]
+    line(1)
+    plane(0)
+    plane(1)
+
+    unpack(0, state_grad)
     state_grad_16 = state_grad[...].astype(BF16)
     values_grad[...] += fall[...] * dot(key[...], state_grad_16, 1, 1)
     rounded[...] = values_grad[...].astype(BF16)
@@ -281,53 +340,60 @@
         return axes[a][8][way][s, span(a, c), :]
 
     def finish_queries():
-        arrived(first(in_f), scan_recv.at[3])
-        before = jnp.concatenate([in_f[:, h, :] for h in range(heads)], axis=0)
-        query_grad[...] = local_q[...] + dot(grad_rise[...], before.astype(BF16), 1, 0)
+        unpack(1, before)
+        query_grad[...] = local_q[...] + dot(grad_rise[...], before[...].astype(BF16), 1, 0)
 
     def finish_keys():
         key_grad[...] = local_k[...] + dot(value_fall[...], state_grad[...].astype(BF16), 1, 0)
 
+    def mixer_change():
+        whole = mixed[...] + rise[...] * dot(query[...], before[...].astype(BF16), 1, 1)
+        mixed[...] = grad[...].astype(F32) * whole - value[...].astype(F32) * values_grad[...]
+
     def finish_decays():
-        before = jnp.concatenate([in_f[:, h, :] for h in range(heads)], axis=0)
-        whole = mixed[...] + rise[...] * dot(query[...], before.astype(BF16), 1, 1)
-        change = grad[...].astype(F32) * whole - value[...].astype(F32) * values_grad[...]
         owner = lax.broadcasted_iota(jnp.int32, (8, width), 1) // depth
         pick = jnp.where(owner == lax.broadcasted_iota(jnp.int32, (8, width), 0), 1.0, 0.0).astype(BF16)
-        by_head = sum(dot(pick, part, 1, 1) for part in thirds(change))
+        by_head = sum(dot(pick, part, 1, 1) for part in thirds(mixed[...]))
         through = unstacked(dot(stacked(by_head), tri[...], 1, 1))
-        row = lax.broadcasted_iota(jnp.int32, (8, 1), 0)
-        beyond = jnp.zeros((8, 1), F32)
+        decay_grad[...] = through[0:heads, :]
+
+    def add_beyond():
+        row = lax.broadcasted_iota(jnp.int32, (heads, 1), 0)
+        beyond = jnp.zeros((heads, 1), F32)
         for h in range(heads):
             part = slice(h * depth, (h + 1) * depth)
-            end = before[part] * jnp.exp(down[rows - 1 : rows, h : h + 1]) + own_state[part, :]
+            end = before[part, :] * jnp.exp(down[rows - 1 : rows, h : h + 1]) + own_state[part, :]
             flow = jnp.sum(jnp.sum(end * state_grad[part, :], axis=0, keepdims=True), axis=1, keepdims=True)
             beyond = jnp.where(row == h, flow, beyond)
-        decay_grad[...] = (through + beyond)[0:heads, :]
-
-    extra = [finish_queries, finish_keys, finish_decays]
+        decay_grad[...] += beyond
+
+    def products(s):
+        if s == reach:
+            return [functools.partial(product, a, 0) for a in range(2)]
+        return [functools.partial(product, a, block_of(a, way, s)) for a in range(2) for way in range(2)]
+
+    gaps = [work for s in range(3, reach + 1) for work in products(s)]
+    gaps += [finish_queries, finish_keys, mixer_change, finish_decays, add_beyond]
+    order = per_piece(ny)
     for a in range(2):
         product(a, reach)
-    for c in ORDER:
-        for a in range(2):
+        for c in order:
             for way in range(2):
                 if comes(way, 0, c):
                     hop(a, way, 0, c)
+    for s in range(1, 3):
+        for work in products(s):
+            work()
     for s in range(1, reach):
-        for a in range(2):
-            for way in range(2):
-                product(a, block_of(a, way, s))
-        if s > 1 and extra:
-            extra.pop(0)()
-        for c in ORDER:
+        for i, c in enumerate(order):
             for a in range(2):
                 for way in range(2):
                     if comes(way, s - 1, c):
                         axes[a][7][block_of(a, way, s), span(a, c), :] += landed(a, way, s - 1, c)
                     hop(a, way, s, c)
-    for a in range(2):
-        product(a, 0)
-    for c in ORDER:
+            if i % 2 and gaps:
+                gaps.pop(0)()
+    for c in order:
         for a in range(2):
             _, _, _, name_o, n_o, at_o, _, partial, _, block, last = axes[a]
             block[span(a, c), :] = partial[0, span(a, c), :] + landed(a, 0, reach - 1, c) + landed(a, 1, reach - 1, c)
@@ -341,7 +407,7 @@
                         src_ref=block.at[part], dst_ref=last.at[j], send_sem=last_send.at[a], recv_sem=last_recv.at[a],
                         device_id={name_o: lax.rem(at_o + j, n_o)}, device_id_type=MESH,
                     ).start()
-    for work in extra:
+    for work in gaps:
         work()
 
     squares = jnp.zeros((small, pair), F32)
@@ -369,14 +435,28 @@
         sums += norm_in[j]
     norms[...] = sums[0:1, 0:small]
 
-    for i, buffer in enumerate((send_b, send_f, out_b, out_f)):
-        arrived(first(buffer), scan_send.at[i])
+    arrived(all_but_one(logs), log_send.at[0])
+    arrived(all_but_one(row_logs), log_send.at[1])
+    for number in range(2):
+        arrived(all_but_one(scan_send_buf.at[number]), scan_send.at[number, 0])
+        each_row(number, True, row_send_sem)
+        arrived(all_but_one(scan_out.at[number]), scan_send.at[number, 2])
     for a in range(2):
         n, n_o, partial, last = axes[a][1], axes[a][4], axes[a][7], axes[a][10]
         arrived(partial.at[pl.ds(0, n - 1)], ring_send.at[a])
         arrived(last.at[pl.ds(1, n_o - 1)], last_send.at[a])
     if nt > 1:
         arrived(norm_in.at[pl.ds(1, nt - 1)], norm_send)
+
+
+def put_out(*refs):
+    *sources, sems = refs
+    count = len(sources) // 2
+    copies = [pltpu.make_async_copy(sources[i], sources[count + i], sems.at[i]) for i in range(count)]
+    for copy in copies:
+        copy.start()
+    for copy in copies:
+        copy.wait()
 
 
 def on_device(nz, ny, nt, block_input, value_weight, queries, key_rows, log_decay, out_grad):
@@ -386,6 +466,7 @@
     pair = 2 * (width // heads)
     reach = nz // 2
     tall_a, tall_b, small = model // nz, model // ny, model // shards
+    tiles = width // heads // ny
     vmem, dma = pltpu.VMEM, pltpu.SemaphoreType.DMA
     shape = jax.ShapeDtypeStruct
     scratch = [
@@ -394,22 +475,25 @@
         vmem((rows, width), BF16), vmem((heads, rows, pair), BF16), vmem((heads, rows, pair), BF16),
         vmem((rows, width), F32), vmem((rows, width), F32), vmem((rows, width), BF16), vmem((rows, width), BF16),
         vmem((rows, rows), BF16), vmem((rows, 128), F32), vmem((8, rows), F32),
-        vmem((shards, 8, state), F32), vmem((shards, 8, state), F32), vmem((shards, heads, state), F32), vmem((shards, heads, state), F32),
-        vmem((shards, heads, state), F32), vmem((shards, heads, state), F32), vmem((shards, heads, state), F32), vmem((shards, heads, state), F32),
+        vmem((ny, 1, 128), F32), vmem((nz, 1, 128), F32),
+        vmem((2, ny, heads, tiles, state), F32), vmem((2, ny, heads, tiles, state), F32),
+        vmem((2, heads, tiles, state), F32), vmem((2, nz, heads, tiles, state), F32),
+        vmem((2, ny, heads, tiles, state), F32), vmem((2, ny, heads, tiles, state), F32), vmem((nz, heads, tiles, state), F32),
+        vmem((width, state), F32),
         vmem((width, state), F32), vmem((width, state), F32), vmem((rows, width), F32), vmem((rows, width), F32),
         vmem((rows, state), F32), vmem((rows, state), F32), vmem((rows, width), BF16),
         vmem((nz, tall_a, rows), BF16), vmem((ny, tall_b, rows), BF16), vmem((nz, tall_a, pair), F32), vmem((ny, tall_b, pair), F32),
         vmem((reach, tall_a, pair), F32), vmem((reach, tall_a, pair), F32), vmem((reach, tall_b, pair), F32), vmem((reach, tall_b, pair), F32),
         vmem((tall_a, pair), F32), vmem((tall_b, pair), F32), vmem((ny, small, pair), F32), vmem((nz, small, pair), F32),
         vmem((8, 128), F32), vmem((nt, 8, 128), F32),
-        dma((5 + LOADS,)), dma((4,)), dma((4,)), dma((2,)), dma((4 * reach * CHUNKS,)), dma((2,)), dma((2,)), dma, dma,
+        dma((5 + LOADS,)), dma((2,)), dma((2,)), dma((2, nz)), dma((2, nz)), dma((2, 3)), dma((2, 3)), dma((2,)), dma((4 * reach * CHUNKS,)), dma((2,)), dma((2,)), dma, dma,
     ]
-    query_grad, key_grad, decay_grad, weight_grad, norms = pl.pallas_call(
+    results = (
+        ((rows, state), F32), ((rows, state), F32), ((heads, rows), F32), ((small, width), F32), ((1, small), F32)
+    )
+    kept = pl.pallas_call(
         functools.partial(kernel, nz, ny, nt),
-        out_shape=(
-            shape((rows, state), F32), shape((rows, state), F32), shape((heads, rows), F32),
-            shape((small, width), F32), shape((1, small), F32),
-        ),
+        out_shape=tuple(vmem(*each) for each in results),
         in_specs=[pl.BlockSpec(memory_space=pl.ANY)] * 6,
         out_specs=(pl.BlockSpec(memory_space=pltpu.VMEM),) * 5,
         scratch_shapes=scratch,
@@ -417,6 +501,13 @@
             collective_id=0, has_side_effects=True, vmem_limit_bytes=56 * 1024 * 1024
         ),
     )(log_decay.T, out_grad, queries, key_rows, block_input, value_weight)
+    query_grad, key_grad, decay_grad, weight_grad, norms = pl.pallas_call(
+        put_out,
+        out_shape=tuple(shape(*each) for each in results),
+        in_specs=[pl.BlockSpec(memory_space=pltpu.VMEM)] * 5,
+        out_specs=(pl.BlockSpec(memory_space=pl.ANY),) * 5,
+        scratch_shapes=[dma((5,))],
+    )(*(pltpu.with_memory_space_constraint(each, pltpu.VMEM) for each in kept))
     return query_grad, key_grad, decay_grad.T, weight_grad, norms.reshape(small)
 
 

time: 71.8 us -> 60 us (0.84)
  local copies, waits for them, and re-layouts: 7.11 us -> 0 us
  Pallas kernels: 63.8 us -> 59.2 us
    unnamed x5 -> x0, local copies, waits for them, and re-layouts: 7.11 us -> none
    pallas_call x1 -> x2, Pallas kernels: 63.8 us -> 59.2 us  [the longest x1 58.4 us: on_device(): pl.pallas_call(functools.partial(kernel, nz, ny, nt), out_shape=tuple((vm...]
where the time goes in v2:
time: 60 us; the launch traced here: 59.9 us
  Pallas kernels  59.2 us (99%)
  between operations  0.64 us (1%)
    pallas_call x1, Pallas kernels, on_device(): pl.pallas_call(functools.partial(kernel, nz, ny, nt), out_shape=tuple((vm...  58.4 us

profile of v2, /device:TPU:1, one launch (start us, length us, event | category | flops | bytes accessed | tf_op | source)
XLA Modules:
  0.0 59.9 jit_solution(2812844272020330599)
XLA Ops:
  0.6 58.4 %shard_map.101 = (f32[512,128]{1,0:T(8,128)S(1)}, f32[512,128]{1,0:T(8,128)S(1)}, f32[4,512]{1,0:T(4,128)S(1)}, f32[32,256]{1,0:T(8,128)S(1)}, f32[1,32]{1,0:T(1,128)S(1)}) custom-call(f32[4,512]{1,0:T(4,128)} %bitcast.3, bf16[512,256]{1,0:T(8,128)(2,1)} %grad_hbm.1, bf16[512,128]{1,0:T(8,128)(2,1)} %query_hbm.1, bf16[512,128]{1,0:T(8,128)(2,1)} %key_hbm.1, ...), custom_call_target="tpu_custom_call" | custom-call | tf_op jit(solution)/shard_map/pallas_call | solution.py:494
  59.0 0.8 %shard_map.102 = (f32[512,128]{1,0:T(8,128)}, f32[512,128]{1,0:T(8,128)}, f32[4,512]{1,0:T(4,128)}, f32[32,256]{1,0:T(8,128)}, f32[1,32]{1,0:T(1,128)}) custom-call(f32[512,128]{1,0:T(8,128)S(1)} %get-tuple-element.15.refs_0_, f32[512,128]{1,0:T(8,128)S(1)} %get-tuple-element.16.refs_1_, f32[4,512]{1,0:T(4,128)S(1)} %get-tuple-element.17.refs_2_, ...), custom_call_target="tpu_custom_call" | custom-call | tf_op jit(solution)/shard_map/pallas_call | solution.py:504

commit v3 on v2

--- a/solution.py
+++ b/solution.py
@@ -13,6 +13,7 @@
 BF16 = jnp.bfloat16
 MESH = pl.DeviceIdType.MESH
 LOADS = 4
+PARTS = 2
 CHUNKS = 8
 
 
@@ -130,21 +131,24 @@
     grad_rise[...] = (grad[...].astype(F32) * rise[...]).astype(BF16)
     tiles = depth // ny
 
+    group = heads // PARTS
+
     def pack(number, own):
         for g in range(ny):
             for h in range(heads):
                 at = h * depth + g * tiles
-                scan_send_buf[number, g, h] = own[at : at + tiles, :]
+                scan_send_buf[number, h // group, g, h % group] = own[at : at + tiles, :]
 
     pack(0, dot(grad_rise[...], query[...], 0, 0))
     logs[y] = down[rows - 1 : rows, :]
 
     def first_round(number):
-        along(
-            "sp_1", lambda other: scan_send_buf.at[number, other], scan_recv_buf.at[number, y],
-            scan_send.at[number, 0], scan_recv.at[number, 0],
-        )
-        scan_recv_buf[number, y] = scan_send_buf[number, y]
+        for p in range(PARTS):
+            along(
+                "sp_1", lambda other: scan_send_buf.at[number, p, other], scan_recv_buf.at[number, p, y],
+                scan_send.at[number, 0, p], scan_recv.at[number, 0, p],
+            )
+            scan_recv_buf[number, p, y] = scan_send_buf[number, p, y]
 
     pl.semaphore_wait(barrier, nz - 1 + ny - 1 + nt - 1)
     along("sp_1", lambda other: logs.at[y], logs.at[y], log_send.at[0], log_recv.at[0])
@@ -173,6 +177,81 @@
         mine = (lane < depth) if h % 2 == 0 else (lane >= depth)
         grad_of[h] = jnp.where(mine, grad[:, cols].astype(F32), 0.0).astype(BF16)
         value_of[h] = jnp.where(mine, value[:, cols].astype(F32), 0.0).astype(BF16)
+
+    arrived(all_but_one(logs), log_recv.at[0])
+    line_logs = [logs[k] for k in range(ny)]
+    row_logs[z] = sum(line_logs[1:], line_logs[0])
+    along("sp_0", lambda other: row_logs.at[z], row_logs.at[z], log_send.at[1], log_recv.at[1])
+
+    def splat(row):
+        return [jnp.broadcast_to(row[:, h : h + 1], (tiles, state)) for h in range(heads)]
+
+    factors = [splat(jnp.exp(row)) for row in line_logs]
+
+    def steps(number, n):
+        return list(range(n)) if number else list(reversed(range(n)))
+
+    def row_copy(number, p, to, slot, sem):
+        return pltpu.make_async_remote_copy(
+            src_ref=row_send.at[number, p], dst_ref=row_recv.at[number, p, slot],
+            send_sem=row_send_sem.at[number, p, sem], recv_sem=row_recv_sem.at[number, p, slot],
+            device_id={"sp_0": to}, device_id_type=MESH,
+        )
+
+    def each_row(number, p, sent, sem):
+        for k in range(nz):
+
+            @pl.when(k > z if bool(number) == sent else k < z)
+            def _():
+                arrived(row_recv.at[number, p, k], sem.at[number, p, k])
+
+    def line(number, p):
+        arrived(all_but_one(scan_recv_buf.at[number, p]), scan_recv.at[number, 0, p])
+        total = [jnp.zeros((tiles, state), F32) for _ in range(group)]
+        for k in steps(number, ny):
+            for h in range(group):
+                scan_out[number, p, k, h] = total[h]
+                total[h] = factors[k][p * group + h] * total[h] + scan_recv_buf[number, p, k, h]
+        for h in range(group):
+            row_send[number, p, h] = total[h]
+        for d in range(1, nz):
+            other = z + d if number else z - d
+            inside = other < nz if number else other >= 0
+
+            @pl.when(inside)
+            def _():
+                row_copy(number, p, other, z, other).start()
+
+    def line_factors(k):
+        return splat(jnp.exp(row_logs[k]))
+
+    def plane(number, p):
+        each_row(number, p, False, row_recv_sem)
+        total = [jnp.zeros((tiles, state), F32) for _ in range(group)]
+        for k in steps(number, nz):
+            for h in range(group):
+                beyond_rows[number, p, k, h] = total[h]
+                total[h] = whole_factors[k][p * group + h] * total[h] + row_recv[number, p, k, h]
+        reaching = [beyond_rows[number, p, z, h] for h in range(group)]
+        for k in steps(number, ny):
+            for h in range(group):
+                scan_out[number, p, k, h] += reaching[h]
+                reaching[h] = factors[k][p * group + h] * reaching[h]
+        scan_in[number, p, y] = scan_out[number, p, y]
+        along(
+            "sp_1", lambda other: scan_out.at[number, p, other], scan_in.at[number, p, y],
+            scan_send.at[number, 1, p], scan_recv.at[number, 1, p],
+        )
+
+    def unpack(number, p, target):
+        arrived(all_but_one(scan_in.at[number, p]), scan_recv.at[number, 1, p])
+        for g in range(ny):
+            for h in range(group):
+                at = (p * group + h) * depth + g * tiles
+                target[at : at + tiles, :] = scan_in[number, p, g, h]
+
+    for p in range(PARTS):
+        line(0, p)
 
     half = rows // 2
     causal = lax.broadcasted_iota(jnp.int32, (half, half), 0) >= lax.broadcasted_iota(jnp.int32, (half, half), 1)
@@ -216,89 +295,19 @@
         else:
             local_k[of, :] += to_k
 
-    arrived(all_but_one(logs), log_recv.at[0])
-    line_logs = [logs[k] for k in range(ny)]
-    row_logs[z] = sum(line_logs[1:], line_logs[0])
-    along("sp_0", lambda other: row_logs.at[z], row_logs.at[z], log_send.at[1], log_recv.at[1])
-
-    def splat(row):
-        return [jnp.broadcast_to(row[:, h : h + 1], (tiles, state)) for h in range(heads)]
-
-    factors = [splat(jnp.exp(row)) for row in line_logs]
-
-    def steps(number, n):
-        return list(range(n)) if number else list(reversed(range(n)))
-
-    def row_copy(number, to, slot, sem):
-        return pltpu.make_async_remote_copy(
-            src_ref=row_send.at[number], dst_ref=row_recv.at[number, slot],
-            send_sem=row_send_sem.at[number, sem], recv_sem=row_recv_sem.at[number, slot],
-            device_id={"sp_0": to}, device_id_type=MESH,
-        )
-
-    def each_row(number, sent, sem):
-        for k in range(nz):
-
-            @pl.when(k > z if bool(number) == sent else k < z)
-            def _():
-                arrived(row_recv.at[number, k], sem.at[number, k])
-
-    def line(number):
-        arrived(all_but_one(scan_recv_buf.at[number]), scan_recv.at[number, 0])
-        total = [jnp.zeros((tiles, state), F32) for _ in range(heads)]
-        for k in steps(number, ny):
-            for h in range(heads):
-                scan_out[number, k, h] = total[h]
-                total[h] = factors[k][h] * total[h] + scan_recv_buf[number, k, h]
-        for h in range(heads):
-            row_send[number, h] = total[h]
-        for d in range(1, nz):
-            other = z + d if number else z - d
-            inside = other < nz if number else other >= 0
-
-            @pl.when(inside)
-            def _():
-                row_copy(number, other, z, other).start()
-
-    def line_factors(k):
-        return splat(jnp.exp(row_logs[k]))
-
-    def plane(number):
-        each_row(number, False, row_recv_sem)
-        total = [jnp.zeros((tiles, state), F32) for _ in range(heads)]
-        for k in steps(number, nz):
-            for h in range(heads):
-                beyond_rows[k, h] = total[h]
-                total[h] = whole_factors[k][h] * total[h] + row_recv[number, k, h]
-        reaching = [beyond_rows[z, h] for h in range(heads)]
-        for k in steps(number, ny):
-            for h in range(heads):
-                scan_out[number, k, h] += reaching[h]
-                reaching[h] = factors[k][h] * reaching[h]
-        scan_in[number, y] = scan_out[number, y]
-        along(
-            "sp_1", lambda other: scan_out.at[number, other], scan_in.at[number, y],
-            scan_send.at[number, 2], scan_recv.at[number, 2],
-        )
-
-    def unpack(number, target):
-        arrived(all_but_one(scan_in.at[number]), scan_recv.at[number, 2])
-        for g in range(ny):
-            for h in range(heads):
-                at = h * depth + g * tiles
-                target[at : at + tiles, :] = scan_in[number, g, h]
-
-    line(0)
     arrived(all_but_one(row_logs), log_recv.at[1])
     whole_factors = [line_factors(k) for k in range(nz)]
-    line(1)
-    plane(0)
-    plane(1)
-
-    unpack(0, state_grad)
-    state_grad_16 = state_grad[...].astype(BF16)
-    values_grad[...] += fall[...] * dot(key[...], state_grad_16, 1, 1)
-    rounded[...] = values_grad[...].astype(BF16)
+    for p in range(PARTS):
+        line(1, p)
+    for p in range(PARTS):
+        plane(0, p)
+
+    def value_half(a):
+        for p in range(a * PARTS // 2, (a + 1) * PARTS // 2):
+            unpack(0, p, state_grad)
+        cols = slice(a * pair, (a + 1) * pair)
+        values_grad[:, cols] += fall[:, cols] * dot(key[...], state_grad[cols, :].astype(BF16), 1, 1)
+        rounded[:, cols] = values_grad[:, cols].astype(BF16)
 
     axes = (
         ("sp_0", nz, z, "sp_1", ny, y, turned_a, partial_a, (ring_ap, ring_am), block_a, last_a),
@@ -340,7 +349,8 @@
         return axes[a][8][way][s, span(a, c), :]
 
     def finish_queries():
-        unpack(1, before)
+        for p in range(PARTS):
+            unpack(1, p, before)
         query_grad[...] = local_q[...] + dot(grad_rise[...], before[...].astype(BF16), 1, 0)
 
     def finish_keys():
@@ -368,31 +378,37 @@
         decay_grad[...] += beyond
 
     def products(s):
-        if s == reach:
-            return [functools.partial(product, a, 0) for a in range(2)]
-        return [functools.partial(product, a, block_of(a, way, s)) for a in range(2) for way in range(2)]
-
-    gaps = [work for s in range(3, reach + 1) for work in products(s)]
-    gaps += [finish_queries, finish_keys, mixer_change, finish_decays, add_beyond]
+        for a in range(2):
+            for way in range(2 if 0 < s < reach else 1):
+                product(a, block_of(a, way, s) if s < reach else 0)
+
     order = per_piece(ny)
     for a in range(2):
+        value_half(a)
         product(a, reach)
         for c in order:
             for way in range(2):
                 if comes(way, 0, c):
                     hop(a, way, 0, c)
-    for s in range(1, 3):
-        for work in products(s):
-            work()
+    products(1)
+    if reach > 2:
+        products(2)
+    for p in range(PARTS):
+        plane(1, p)
     for s in range(1, reach):
-        for i, c in enumerate(order):
+        for c in order:
             for a in range(2):
                 for way in range(2):
                     if comes(way, s - 1, c):
                         axes[a][7][block_of(a, way, s), span(a, c), :] += landed(a, way, s - 1, c)
                     hop(a, way, s, c)
-            if i % 2 and gaps:
-                gaps.pop(0)()
+        if s + 2 <= reach:
+            products(s + 2)
+        elif reach == 2:
+            products(2)
+        if s == max(reach - 2, 1):
+            finish_keys()
+    finish_queries()
     for c in order:
         for a in range(2):
             _, _, _, name_o, n_o, at_o, _, partial, _, block, last = axes[a]
@@ -407,8 +423,9 @@
                         src_ref=block.at[part], dst_ref=last.at[j], send_sem=last_send.at[a], recv_sem=last_recv.at[a],
                         device_id={name_o: lax.rem(at_o + j, n_o)}, device_id_type=MESH,
                     ).start()
-    for work in gaps:
-        work()
+    mixer_change()
+    finish_decays()
+    add_beyond()
 
     squares = jnp.zeros((small, pair), F32)
     for a in range(2):
@@ -438,9 +455,10 @@
     arrived(all_but_one(logs), log_send.at[0])
     arrived(all_but_one(row_logs), log_send.at[1])
     for number in range(2):
-        arrived(all_but_one(scan_send_buf.at[number]), scan_send.at[number, 0])
-        each_row(number, True, row_send_sem)
-        arrived(all_but_one(scan_out.at[number]), scan_send.at[number, 2])
+        for p in range(PARTS):
+            arrived(all_but_one(scan_send_buf.at[number, p]), scan_send.at[number, 0, p])
+            each_row(number, p, True, row_send_sem)
+            arrived(all_but_one(scan_out.at[number, p]), scan_send.at[number, 1, p])
     for a in range(2):
         n, n_o, partial, last = axes[a][1], axes[a][4], axes[a][7], axes[a][10]
         arrived(partial.at[pl.ds(0, n - 1)], ring_send.at[a])
@@ -466,7 +484,7 @@
     pair = 2 * (width // heads)
     reach = nz // 2
     tall_a, tall_b, small = model // nz, model // ny, model // shards
-    tiles = width // heads // ny
+    tiles, group = width // heads // ny, heads // PARTS
     vmem, dma = pltpu.VMEM, pltpu.SemaphoreType.DMA
     shape = jax.ShapeDtypeStruct
     scratch = [
@@ -476,9 +494,10 @@
         vmem((rows, width), F32), vmem((rows, width), F32), vmem((rows, width), BF16), vmem((rows, width), BF16),
         vmem((rows, rows), BF16), vmem((rows, 128), F32), vmem((8, rows), F32),
         vmem((ny, 1, 128), F32), vmem((nz, 1, 128), F32),
-        vmem((2, ny, heads, tiles, state), F32), vmem((2, ny, heads, tiles, state), F32),
-        vmem((2, heads, tiles, state), F32), vmem((2, nz, heads, tiles, state), F32),
-        vmem((2, ny, heads, tiles, state), F32), vmem((2, ny, heads, tiles, state), F32), vmem((nz, heads, tiles, state), F32),
+        vmem((2, PARTS, ny, group, tiles, state), F32), vmem((2, PARTS, ny, group, tiles, state), F32),
+        vmem((2, PARTS, group, tiles, state), F32), vmem((2, PARTS, nz, group, tiles, state), F32),
+        vmem((2, PARTS, ny, group, tiles, state), F32), vmem((2, PARTS, ny, group, tiles, state), F32),
+        vmem((2, PARTS, nz, group, tiles, state), F32),
         vmem((width, state), F32),
         vmem((width, state), F32), vmem((width, state), F32), vmem((rows, width), F32), vmem((rows, width), F32),
         vmem((rows, state), F32), vmem((rows, state), F32), vmem((rows, width), BF16),
@@ -486,7 +505,7 @@
         vmem((reach, tall_a, pair), F32), vmem((reach, tall_a, pair), F32), vmem((reach, tall_b, pair), F32), vmem((reach, tall_b, pair), F32),
         vmem((tall_a, pair), F32), vmem((tall_b, pair), F32), vmem((ny, small, pair), F32), vmem((nz, small, pair), F32),
         vmem((8, 128), F32), vmem((nt, 8, 128), F32),
-        dma((5 + LOADS,)), dma((2,)), dma((2,)), dma((2, nz)), dma((2, nz)), dma((2, 3)), dma((2, 3)), dma((2,)), dma((4 * reach * CHUNKS,)), dma((2,)), dma((2,)), dma, dma,
+        dma((5 + LOADS,)), dma((2,)), dma((2,)), dma((2, PARTS, nz)), dma((2, PARTS, nz)), dma((2, 2, PARTS)), dma((2, 2, PARTS)), dma((2,)), dma((4 * reach * CHUNKS,)), dma((2,)), dma((2,)), dma, dma,
     ]
     results = (
         ((rows, state), F32), ((rows, state), F32), ((heads, rows), F32), ((small, width), F32), ((1, small), F32)

time: 60 us -> 58.3 us (0.972)
  Pallas kernels: 59.2 us -> 57.5 us
    pallas_call x1, Pallas kernels: 58.4 us -> 56.6 us  [on_device(): pl.pallas_call(functools.partial(kernel, nz, ny, nt), out_shape=tuple((vm...]
where the time goes in v3:
time: 58.3 us; the launch traced here: 58.1 us
  Pallas kernels  57.5 us (99%)
  between operations  0.64 us (1%)
    pallas_call x1, Pallas kernels, on_device(): pl.pallas_call(functools.partial(kernel, nz, ny, nt), out_shape=tuple((vm...  56.6 us

profile of v3, /device:TPU:1, one launch (start us, length us, event | category | flops | bytes accessed | tf_op | source)
XLA Modules:
  0.0 58.1 jit_solution(5561119960925532669)
XLA Ops:
  0.6 56.6 %shard_map.101 = (f32[512,128]{1,0:T(8,128)S(1)}, f32[512,128]{1,0:T(8,128)S(1)}, f32[4,512]{1,0:T(4,128)S(1)}, f32[32,256]{1,0:T(8,128)S(1)}, f32[1,32]{1,0:T(1,128)S(1)}) custom-call(f32[4,512]{1,0:T(4,128)} %bitcast.3, bf16[512,256]{1,0:T(8,128)(2,1)} %grad_hbm.1, bf16[512,128]{1,0:T(8,128)(2,1)} %query_hbm.1, bf16[512,128]{1,0:T(8,128)(2,1)} %key_hbm.1, ...), custom_call_target="tpu_custom_call" | custom-call | tf_op jit(solution)/shard_map/pallas_call | solution.py:513
  57.3 0.8 %shard_map.102 = (f32[512,128]{1,0:T(8,128)}, f32[512,128]{1,0:T(8,128)}, f32[4,512]{1,0:T(4,128)}, f32[32,256]{1,0:T(8,128)}, f32[1,32]{1,0:T(1,128)}) custom-call(f32[512,128]{1,0:T(8,128)S(1)} %get-tuple-element.15.refs_0_, f32[512,128]{1,0:T(8,128)S(1)} %get-tuple-element.16.refs_1_, f32[4,512]{1,0:T(4,128)S(1)} %get-tuple-element.17.refs_2_, ...), custom_call_target="tpu_custom_call" | custom-call | tf_op jit(solution)/shard_map/pallas_call | solution.py:523

commit v4 on v3

--- a/solution.py
+++ b/solution.py
@@ -191,19 +191,20 @@
     def steps(number, n):
         return list(range(n)) if number else list(reversed(range(n)))
 
-    def row_copy(number, p, to, slot, sem):
+    def row_copy(number, p, to):
         return pltpu.make_async_remote_copy(
-            src_ref=row_send.at[number, p], dst_ref=row_recv.at[number, p, slot],
-            send_sem=row_send_sem.at[number, p, sem], recv_sem=row_recv_sem.at[number, p, slot],
+            src_ref=row_send.at[number, p], dst_ref=row_recv.at[number, p, z],
+            send_sem=row_send_sem.at[number, p], recv_sem=row_recv_sem.at[number, p],
             device_id={"sp_0": to}, device_id_type=MESH,
         )
 
     def each_row(number, p, sent, sem):
-        for k in range(nz):
-
-            @pl.when(k > z if bool(number) == sent else k < z)
+        count = nz - 1 - z if bool(number) == sent else z
+        for k in range(1, nz):
+
+            @pl.when(count == k)
             def _():
-                arrived(row_recv.at[number, p, k], sem.at[number, p, k])
+                arrived(row_recv.at[number, p, pl.ds(0, k)], sem.at[number, p])
 
     def line(number, p):
         arrived(all_but_one(scan_recv_buf.at[number, p]), scan_recv.at[number, 0, p])
@@ -220,7 +221,7 @@
 
             @pl.when(inside)
             def _():
-                row_copy(number, p, other, z, other).start()
+                row_copy(number, p, other).start()
 
     def line_factors(k):
         return splat(jnp.exp(row_logs[k]))
@@ -325,8 +326,8 @@
     def comes(way, s, c):
         return s > 0 or (c < CHUNKS // 2) == (way == 0)
 
-    def slot(a, way, s, c):
-        return ((a * 2 + way) * reach + s) * CHUNKS + c
+    def slot(s, c):
+        return s * CHUNKS + c
 
     def span(a, c):
         tall = axes[a][7].shape[1] // CHUNKS
@@ -340,12 +341,15 @@
         name, n, at, _, _, _, _, partial, ring, _, _ = axes[a]
         pltpu.make_async_remote_copy(
             src_ref=partial.at[block_of(a, way, s), span(a, c)], dst_ref=ring[way].at[s, span(a, c)],
-            send_sem=ring_send.at[a], recv_sem=ring_recv.at[slot(a, way, s, c)],
+            send_sem=ring_send.at[a], recv_sem=ring_recv.at[slot(s, c)],
             device_id={name: lax.rem(at + (1 if way == 0 else n - 1), n)}, device_id_type=MESH,
         ).start()
 
+    def all_landed(s, c):
+        flows = 2 * sum(comes(way, s, c) for way in range(2))
+        arrived(axes[0][8][0].at[s, pl.ds(0, flows * (tall_a // CHUNKS))], ring_recv.at[slot(s, c)])
+
     def landed(a, way, s, c):
-        arrived(axes[a][8][way].at[s, span(a, c)], ring_recv.at[slot(a, way, s, c)])
         return axes[a][8][way][s, span(a, c), :]
 
     def finish_queries():
@@ -397,6 +401,7 @@
         plane(1, p)
     for s in range(1, reach):
         for c in order:
+            all_landed(s - 1, c)
             for a in range(2):
                 for way in range(2):
                     if comes(way, s - 1, c):
@@ -410,6 +415,7 @@
             finish_keys()
     finish_queries()
     for c in order:
+        all_landed(reach - 1, c)
         for a in range(2):
             _, _, _, name_o, n_o, at_o, _, partial, _, block, last = axes[a]
             block[span(a, c), :] = partial[0, span(a, c), :] + landed(a, 0, reach - 1, c) + landed(a, 1, reach - 1, c)
@@ -505,7 +511,7 @@
         vmem((reach, tall_a, pair), F32), vmem((reach, tall_a, pair), F32), vmem((reach, tall_b, pair), F32), vmem((reach, tall_b, pair), F32),
         vmem((tall_a, pair), F32), vmem((tall_b, pair), F32), vmem((ny, small, pair), F32), vmem((nz, small, pair), F32),
         vmem((8, 128), F32), vmem((nt, 8, 128), F32),
-        dma((5 + LOADS,)), dma((2,)), dma((2,)), dma((2, PARTS, nz)), dma((2, PARTS, nz)), dma((2, 2, PARTS)), dma((2, 2, PARTS)), dma((2,)), dma((4 * reach * CHUNKS,)), dma((2,)), dma((2,)), dma, dma,
+        dma((5 + LOADS,)), dma((2,)), dma((2,)), dma((2, PARTS)), dma((2, PARTS)), dma((2, 2, PARTS)), dma((2, 2, PARTS)), dma((2,)), dma((reach * CHUNKS,)), dma((2,)), dma((2,)), dma, dma,
     ]
     results = (
         ((rows, state), F32), ((rows, state), F32), ((heads, rows), F32), ((small, width), F32), ((1, small), F32)

time: 58.3 us -> 57 us (0.978)
  Pallas kernels: 57.5 us -> 56.2 us
    pallas_call x1, Pallas kernels: 56.6 us -> 55.4 us  [on_device(): pl.pallas_call(functools.partial(kernel, nz, ny, nt), out_shape=tuple((vm...]
where the time goes in v4:
time: 57 us; the launch traced here: 56.9 us
  Pallas kernels  56.2 us (99%)
  between operations  0.64 us (1%)
    pallas_call x1, Pallas kernels, on_device(): pl.pallas_call(functools.partial(kernel, nz, ny, nt), out_shape=tuple((vm...  55.4 us

profile of v4, /device:TPU:1, one launch (start us, length us, event | category | flops | bytes accessed | tf_op | source)
XLA Modules:
  0.0 56.9 jit_solution(9568663525606420020)
XLA Ops:
  0.6 55.4 %shard_map.101 = (f32[512,128]{1,0:T(8,128)S(1)}, f32[512,128]{1,0:T(8,128)S(1)}, f32[4,512]{1,0:T(4,128)S(1)}, f32[32,256]{1,0:T(8,128)S(1)}, f32[1,32]{1,0:T(1,128)S(1)}) custom-call(f32[4,512]{1,0:T(4,128)} %bitcast.3, bf16[512,256]{1,0:T(8,128)(2,1)} %grad_hbm.1, bf16[512,128]{1,0:T(8,128)(2,1)} %query_hbm.1, bf16[512,128]{1,0:T(8,128)(2,1)} %key_hbm.1, ...), custom_call_target="tpu_custom_call" | custom-call | tf_op jit(solution)/shard_map/pallas_call | solution.py:519
  56.0 0.8 %shard_map.102 = (f32[512,128]{1,0:T(8,128)}, f32[512,128]{1,0:T(8,128)}, f32[4,512]{1,0:T(4,128)}, f32[32,256]{1,0:T(8,128)}, f32[1,32]{1,0:T(1,128)}) custom-call(f32[512,128]{1,0:T(8,128)S(1)} %get-tuple-element.15.refs_0_, f32[512,128]{1,0:T(8,128)S(1)} %get-tuple-element.16.refs_1_, f32[4,512]{1,0:T(4,128)S(1)} %get-tuple-element.17.refs_2_, ...), custom_call_target="tpu_custom_call" | custom-call | tf_op jit(solution)/shard_map/pallas_call | solution.py:529

commit v5 on v4

--- a/solution.py
+++ b/solution.py
@@ -411,9 +411,6 @@
             products(s + 2)
         elif reach == 2:
             products(2)
-        if s == max(reach - 2, 1):
-            finish_keys()
-    finish_queries()
     for c in order:
         all_landed(reach - 1, c)
         for a in range(2):
@@ -429,6 +426,8 @@
                         src_ref=block.at[part], dst_ref=last.at[j], send_sem=last_send.at[a], recv_sem=last_recv.at[a],
                         device_id={name_o: lax.rem(at_o + j, n_o)}, device_id_type=MESH,
                     ).start()
+    finish_keys()
+    finish_queries()
     mixer_change()
     finish_decays()
     add_beyond()

time: 57 us -> 57 us (level)
  no operation moved by 1% of the time
where the time goes in v5:
time: 57 us; the launch traced here: 56.9 us
  Pallas kernels  56.2 us (99%)
  between operations  0.64 us (1%)
    pallas_call x1, Pallas kernels, on_device(): pl.pallas_call(functools.partial(kernel, nz, ny, nt), out_shape=tuple((vm...  55.4 us

profile of v5, /device:TPU:1, one launch (start us, length us, event | category | flops | bytes accessed | tf_op | source)
XLA Modules:
  0.0 56.9 jit_solution(14551495194696661859)
XLA Ops:
  0.6 55.4 %shard_map.101 = (f32[512,128]{1,0:T(8,128)S(1)}, f32[512,128]{1,0:T(8,128)S(1)}, f32[4,512]{1,0:T(4,128)S(1)}, f32[32,256]{1,0:T(8,128)S(1)}, f32[1,32]{1,0:T(1,128)S(1)}) custom-call(f32[4,512]{1,0:T(4,128)} %bitcast.3, bf16[512,256]{1,0:T(8,128)(2,1)} %grad_hbm.1, bf16[512,128]{1,0:T(8,128)(2,1)} %query_hbm.1, bf16[512,128]{1,0:T(8,128)(2,1)} %key_hbm.1, ...), custom_call_target="tpu_custom_call" | custom-call | tf_op jit(solution)/shard_map/pallas_call | solution.py:518
  56.0 0.8 %shard_map.102 = (f32[512,128]{1,0:T(8,128)}, f32[512,128]{1,0:T(8,128)}, f32[4,512]{1,0:T(4,128)}, f32[32,256]{1,0:T(8,128)}, f32[1,32]{1,0:T(1,128)}) custom-call(f32[512,128]{1,0:T(8,128)S(1)} %get-tuple-element.15.refs_0_, f32[512,128]{1,0:T(8,128)S(1)} %get-tuple-element.16.refs_1_, f32[4,512]{1,0:T(4,128)S(1)} %get-tuple-element.17.refs_2_, ...), custom_call_target="tpu_custom_call" | custom-call | tf_op jit(solution)/shard_map/pallas_call | solution.py:528
